TPU v7x, 32 devices: a whole 2x2x4 slice. The times are simulated.
32 devices in a mesh: grp: 2 (over x), ep: 16 (over z, y, core).
Axes of the slice: x: 2, y: 2, z: 4, core: 2. Of those that a mesh axis runs over, the one named last changes fastest.
Arguments:
- tokens: bfloat16 [1024, 2048], P(('grp', 'ep')), parts along dimension 0, may hold values from -6 to 6
- routes: int32 [1024, 4], P(('grp', 'ep')), parts along dimension 0, may hold values from 0 to 15, all different within a row; in each aligned block of 32 rows (0 to 31, 32 to 63, ...) at most 16 rows name the same one
- in_gain: float32 [2048], replicated, may hold values from 0.1 to 1.9
- group_router: float32 [2048, 4], replicated, may hold values from -0.03125 to 0.03125
- expert_router: float32 [2048, 16], replicated, may hold values from -0.03125 to 0.03125
- w_gate: bfloat16 [16, 2048, 512], P('ep'), may hold values from -0.125 to 0.125
- w_up: bfloat16 [16, 2048, 512], P('ep'), may hold values from -0.125 to 0.125
- w_down: bfloat16 [16, 512, 2048], P('ep')
- out_gain: float32 [2048], P('ep'), may hold values from 0.1 to 1.9
Outputs:
- mixed_out: bfloat16 [1024, 2048], P('grp', 'ep'), parts along dimension 0
There are 2 independent parts, one for each index of `grp`. A program takes and returns all parts, laid end to end along the dimension named above; an argument that names none is the same for every part. Nothing has to cross between parts.
Inputs may be any that keep to these rules, and one draw needn't show every extreme that they name: `routes`: each row names 4 different experts; in the rows of one device no expert is named more than 16 times, a bound that some block reaches.
All inputs are finite; a program needn't handle non-finite values.
Results may differ from a plain program's by a relative error of at most 0.0085.
Values may be sent and summed in bfloat16 or wider, within the bound.
A program may use at most 64 MiB of HBM per device.

v0:
```python
import jax
import jax.numpy as jnp
from jax import lax
from jax.sharding import PartitionSpec as P

EPSILON = 1e-06


def normalize(tokens, in_gain):
    values = tokens.astype(jnp.float32)
    scaled = values * lax.rsqrt(jnp.mean(values * values, axis=1, keepdims=True) + EPSILON)
    return (scaled * in_gain).astype(jnp.bfloat16)


def gate_values(normed, routes, group_router, expert_router):
    wide = normed.astype(jnp.float32)
    group_logit = jnp.dot(wide, group_router, precision=lax.Precision.HIGHEST)
    expert_logit = jnp.dot(wide, expert_router, precision=lax.Precision.HIGHEST)
    group_prob = jnp.exp(group_logit) / jnp.sum(jnp.exp(group_logit), axis=1, keepdims=True)
    chosen = jnp.exp(jnp.take_along_axis(expert_logit, routes, axis=1))
    expert_prob = chosen / jnp.sum(chosen, axis=1, keepdims=True)
    per_group = expert_router.shape[1] // group_router.shape[1]
    return jnp.take_along_axis(group_prob, routes // per_group, axis=1) * expert_prob


def slot_order(pairs, experts):
    onehot = (pairs[:, :, None] == jnp.arange(experts, dtype=jnp.int32)).astype(jnp.int32)
    return jnp.sum(onehot * (jnp.cumsum(onehot, axis=1) - 1), axis=2)


def expert_rows(rows, w_gate, w_up, w_down):
    gate = jnp.dot(rows, w_gate[0], preferred_element_type=jnp.float32)
    upward = jnp.dot(rows, w_up[0], preferred_element_type=jnp.float32)
    hidden = (jax.nn.silu(gate) * upward).astype(jnp.bfloat16)
    return jnp.dot(hidden, w_down[0], preferred_element_type=jnp.float32).astype(jnp.bfloat16)


def per_device(
    tokens, routes, in_gain, group_router, expert_router, w_gate, w_up, w_down, out_gain
):
    tok_dev, top_count = routes.shape
    experts = expert_router.shape[1]
    capacity = 2 * tok_dev * top_count // experts
    normed = normalize(tokens, in_gain)
    weights = gate_values(normed, routes, group_router, expert_router)
    flat_route = routes.reshape(-1)
    order_in = slot_order(flat_route[None, :], experts)[0]
    slot_index = flat_route * capacity + order_in
    token_index = jnp.arange(tok_dev * top_count, dtype=jnp.int32) // top_count
    table = jnp.zeros((experts * capacity,), jnp.int32).at[slot_index].set(token_index)
    filled = jnp.zeros((experts * capacity,), jnp.bool_).at[slot_index].set(True)
    outgoing = jnp.where(filled[:, None], normed[table], jnp.zeros((), jnp.bfloat16))
    outgoing = outgoing.reshape(experts, capacity, normed.shape[1])
    arrived = lax.all_to_all(outgoing, "ep", split_axis=0, concat_axis=0, tiled=True)
    flat_rows = arrived.reshape(-1, arrived.shape[2])
    answer = expert_rows(flat_rows, w_gate, w_up, w_down).reshape(arrived.shape)
    returned = lax.all_to_all(answer, "ep", split_axis=0, concat_axis=0, tiled=True)
    pair_rows = returned.reshape(experts * capacity, normed.shape[1])[slot_index]
    weighted = pair_rows.astype(jnp.float32) * weights.reshape(-1)[:, None]
    mixed = jnp.sum(weighted.reshape(tok_dev, top_count, normed.shape[1]), axis=1)
    local_scale = lax.rsqrt(jnp.mean(mixed * mixed, axis=1, keepdims=True) + EPSILON)
    sending = mixed * local_scale
    part = lax.all_to_all(sending, "ep", split_axis=1, concat_axis=0, tiled=True)
    return (part * out_gain).astype(jnp.bfloat16)


def solution(mesh):
    in_specs = (
        P(("grp", "ep"), None),
        P(("grp", "ep"), None),
        P(),
        P(),
        P(),
        P("ep", None, None),
        P("ep", None, None),
        P("ep", None, None),
        P("ep"),
    )
    out_specs = P("grp", "ep")
    return jax.shard_map(
        per_device, mesh=mesh, in_specs=in_specs, out_specs=out_specs, check_vma=False
    )
```

profile of v0, /device:TPU:0, one launch (start us, length us, event | category | flops | bytes accessed | tf_op | source)
XLA Modules:
  0.0 95.3 jit_solution(5114007452190032896)
XLA Ops:
  0.0 0.8 broadcast_multiply_fusion
  0.8 0.8 copy.65
  1.6 1.0 %fusion.18 = f32[32]{0:T(128)S(1)} fusion(bf16[32,2048]{1,0:T(8,128)(2,1)} %param.9), kind=kLoop, calls=%fused_computation.24 | loop fusion | flops 196576 | bytes 131200 | tf_op jit(solution)/shard_map/reduce_sum | solution.py:11
  3.1 0.2 reduce_window_sum.11
  3.2 0.2 select_reduce_fusion
  3.4 1.0 %scatter_custom_fusion.1 = s32[256]{0:T(256)S(1)} fusion(s32[128]{0:T(128)S(1)} %fusion.28, s32[128]{0:T(128)S(1)} %and_select_fusion, s32[]{:T(128)} %constant.70.clone.1), kind=kCustom, calls=%fused_computation.64 | custom fusion | bytes 1028 | tf_op jit(solution)/shard_map/scatter | solution.py:50
  4.4 1.0 %scatter_custom_fusion = pred[256]{0:T(512)(128)(4,1)S(1)} fusion(s32[128]{0:T(128)S(1)} %fusion.28, pred[128]{0:T(512)(128)(4,1)S(1)} %broadcast.205, pred[]{:T(512)} %constant.68.clone.1), kind=kCustom, calls=%fused_computation.59 | custom fusion | bytes 257 | tf_op jit(solution)/shard_map/scatter | solution.py:51
  5.5 1.0 %fusion.20 = bf16[32,2048]{1,0:T(8,128)(2,1)S(1)} fusion(bf16[32,2048]{1,0:T(8,128)(2,1)} %param.9, f32[2048]{0:T(1024)} %param.11, f32[32]{0:T(128)S(1)} %add_rsqrt_fusion.1), kind=kLoop, calls=%fused_computation.26 | loop fusion | flops 262144 | bytes 270464 | tf_op jit(solution)/shard_map/convert_element_type | solution.py:12
  6.5 1.4 %gather_fusion = bf16[256,2048]{1,0:T(8,128)(2,1)S(1)} fusion(bf16[32,2048]{1,0:T(8,128)(2,1)S(1)} %fusion.20, s32[1024]{0:T(1024)S(1)} %pad_clamp_fusion.1), kind=kCustom, calls=%fused_computation | custom fusion | bytes 2098176 | tf_op jit(solution)/shard_map/gather | solution.py:52
  7.9 0.1 broadcast_select_fusion
  8.1 32.0 %all_to_all.26 = bf16[16,16,2048]{2,1,0:T(8,128)(2,1)S(1)} all-to-all(bf16[16,16,2048]{2,1,0:T(8,128)(2,1)S(1)} %broadcast_select_fusion), channel_id=1, replica_groups=mesh['grp'=2,'ep'=16] {'ep'}, dimensions={0} | all-to-all | bytes 2097152 | tf_op jit(solution)/shard_map/all_to_all | solution.py:54
  40.1 1.6 %fusion.3 = f32[256,512]{1,0:T(8,128)} fusion(bf16[256,2048]{1,0:T(8,128)(2,1)S(1)} %bitcast.54, bf16[1,2048,512]{2,1,0:T(8,128)(2,1)S(1)} %copy-done.5), kind=kOutput, calls=%fused_computation.10 | convolution fusion | flops 536870912 | bytes 3670016 | tf_op jit(solution)/shard_map/dot_general | solution.py:32
  41.7 4.0 %convolution_convert_fusion = bf16[256,2048]{1,0:T(8,128)(2,1)} fusion(bf16[1,512,2048]{2,1,0:T(8,128)(2,1)S(1)} %copy-done, bf16[256,2048]{1,0:T(8,128)(2,1)S(1)} %bitcast.55, bf16[1,2048,512]{2,1,0:T(8,128)(2,1)} %param.15, f32[256,512]{1,0:T(8,128)} %fusion.3), kind=kOutput, calls=%fused_computation.6 | convolution fusion | flops 1075052544 | bytes 6815744 | tf_op jit(solution)/shard_map/dot_general | solution.py:35
  45.7 5.2 %all-to-all-start.1 = ((bf16[16,16,2048]{2,1,0:T(8,128)(2,1)}), bf16[16,16,2048]{2,1,0:T(8,128)(2,1)S(1)}, u32[]{:S(2)}, u32[]{:S(2)}) async-start(bf16[16,16,2048]{2,1,0:T(8,128)(2,1)} %bitcast.53), calls=%async_computation.1 | async-start | bytes 2097152 | tf_op jit(solution)/shard_map/all_to_all | solution.py:57
  51.3 0.2 fusion.34
  51.5 1.4 %gather_fusion.3 = f32[128]{0:T(128)S(1)} fusion(f32[32,16]{0,1:T(8,128)S(1)} %fusion.34, s32[128]{0:T(128)S(1)} %reshape.246), kind=kCustom, calls=%fused_computation.3 | custom fusion | bytes 2048 | tf_op jit(solution)/shard_map/jit(take_along_axis)/gather | solution.py:20
  53.0 0.2 fusion.33
  53.3 1.5 %gather_fusion.2 = f32[128]{0:T(128)S(1)} fusion(f32[32,4]{0,1:T(4,128)S(1)} %broadcast_divide_fusion, s32[128]{0:T(128)S(1)} %reshape.240), kind=kCustom, calls=%fused_computation.2 | custom fusion | bytes 2048 | tf_op jit(solution)/shard_map/jit(take_along_axis)/gather | solution.py:23
  55.1 18.6 %all-to-all-done.1 = bf16[16,16,2048]{2,1,0:T(8,128)(2,1)S(1)} async-done(((bf16[16,16,2048]{2,1,0:T(8,128)(2,1)}), bf16[16,16,2048]{2,1,0:T(8,128)(2,1)S(1)}, u32[]{:S(2)}, u32[]{:S(2)}) %all-to-all-start.1) | async-done | bytes 1048608 | tf_op jit(solution)/shard_map/all_to_all | solution.py:57
  73.7 1.7 %gather_fusion.1 = bf16[128,2048]{1,0:T(8,128)(2,1)} fusion(bf16[256,2048]{1,0:T(8,128)(2,1)S(1)} %bitcast.50, s32[1024]{0:T(1024)S(1)} %pad_clamp_fusion), kind=kCustom, calls=%fused_computation.1 | custom fusion | bytes 1049088 | tf_op jit(solution)/shard_map/gather | solution.py:58
  75.5 1.4 %reshape.223 = f32[32,4,2048]{2,1,0:T(4,128)S(1)} reshape(bf16[128,2048]{1,0:T(8,128)(2,1)} %gather_fusion.1) | data formatting | bytes 1572864 | tf_op jit(solution)/shard_map/convert_element_type | solution.py:59
  76.8 0.7 multiply_reduce_fusion
  78.0 16.6 %all_to_all.27 = f32[32,16,128]{2,0,1:T(8,128)S(1)} all-to-all(f32[32,16,128]{2,0,1:T(8,128)S(1)} %copy.71), channel_id=1, replica_groups=mesh['grp'=2,'ep'=16] {'ep'}, dimensions={1} | all-to-all | bytes 524288 | tf_op jit(solution)/shard_map/all_to_all | solution.py:63
  94.6 0.7 fusion.21
  (42 shorter events, 1.8 us)
Async XLA Ops:
  0.0 41.7 %copy-start = (bf16[1,512,2048]{2,1,0:T(8,128)(2,1)S(1)}, bf16[1,512,2048]{2,1,0:T(8,128)(2,1)}, u32[]{:S(2)}) copy-start(bf16[1,512,2048]{2,1,0:T(8,128)(2,1)} %param.16) | copy-start | bytes 6291460
  7.9 32.2 %copy-start.5 = (bf16[1,2048,512]{2,1,0:T(8,128)(2,1)S(1)}, bf16[1,2048,512]{2,1,0:T(8,128)(2,1)}, u32[]{:S(2)}) copy-start(bf16[1,2048,512]{2,1,0:T(8,128)(2,1)} %param.14) | copy-start | bytes 6291460
  45.7 5.2 %copy-start.2 = (s32[32,4]{0,1:T(4,128)S(1)}, s32[32,4]{0,1:T(4,128)}, u32[]{:S(2)}) copy-start(s32[32,4]{0,1:T(4,128)} %param.10) | copy-start | bytes 1540
  45.7 5.6 %copy-start.1 = (f32[2048,16]{0,1:T(8,128)S(1)}, f32[2048,16]{0,1:T(8,128)}, u32[]{:S(2)}) copy-start(f32[2048,16]{0,1:T(8,128)} %param.13) | copy-start | bytes 393220
  45.7 28.0 %all-to-all-start.1 = ((bf16[16,16,2048]{2,1,0:T(8,128)(2,1)}), bf16[16,16,2048]{2,1,0:T(8,128)(2,1)S(1)}, u32[]{:S(2)}, u32[]{:S(2)}) async-start(bf16[16,16,2048]{2,1,0:T(8,128)(2,1)} %bitcast.53), calls=%async_computation.1 | async-start | bytes 2097152 | tf_op jit(solution)/shard_map/all_to_all | solution.py:57
  51.5 1.5 %copy-start.3 = (f32[2048,4]{0,1:T(4,128)S(1)}, f32[2048,4]{0,1:T(4,128)}, u32[]{:S(2)}) copy-start(f32[2048,4]{0,1:T(4,128)} %param.12) | copy-start | bytes 98308
  76.8 17.8 %copy-start.4 = (f32[128]{0:T(128)S(1)}, f32[128]{0:T(128)}, u32[]{:S(2)}) copy-start(f32[128]{0:T(128)} %param.17) | copy-start | bytes 1540
where the time goes:
time: 95.7 us; the launch traced here: 95.3 us
  blocking collectives  48.6 us (51%)
  waiting for transfers between devices  18.6 us (19%)
  local copies, waits for them, and re-layouts  11.5 us (12%)
  matrix products  5.99 us (6%)
  other arithmetic  5.19 us (5%)
  starting transfers between devices  5.15 us (5%)
    all_to_all x1, blocking collectives, per_device(): lax.all_to_all(outgoing, 'ep', split_axis=0, concat_axis=0, tiled=True)  32 us
    all_to_all x1, waiting for transfers between devices, per_device(): lax.all_to_all(answer, 'ep', split_axis=0, concat_axis=0, tiled=True)  18.6 us
    all_to_all x1, blocking collectives, per_device(): lax.all_to_all(sending, 'ep', split_axis=1, concat_axis=0, tiled=True)  16.6 us
    all_to_all x1, starting transfers between devices, per_device(): lax.all_to_all(answer, 'ep', split_axis=0, concat_axis=0, tiled=True)  5.15 us
    dot_general x1, matrix products, expert_rows(): jnp.dot(hidden, w_down[0], preferred_element_type=jnp.float32)  4.01 us
  transfers between devices with their start and end apart: 1, of which 1 were waited for; matrix products, arithmetic and copies ran while one was open for 4% of the time, Pallas kernels for 0%

commit v1 on v0

v1 whole, which is shorter than its diff:
```python
import functools

import jax
import jax.numpy as jnp
from jax import lax
from jax.experimental import pallas as pl
from jax.experimental.pallas import tpu as pltpu
from jax.sharding import PartitionSpec as P

EPSILON = 1e-06
LANES = 128
CORES = 2
HIGH = lax.Precision.HIGHEST
UP, DOWN, SIDE, CORE = 0, 1, 2, 3


def target_of(step, z, depth):
    mirrored = z * 2 > depth - 1
    near = jnp.where(mirrored, depth - 1 - z, z)
    lone = depth - 1 - 2 * near
    paired = step - lone
    apart = near - paired // 2
    far = jnp.where(paired % 2 == 0, near + apart, near - apart)
    found = jnp.where(step < lone, depth - 1 - step, far)
    return jnp.where(mirrored, depth - 1 - found, found)


def kernel(
    n, tokens, routes, in_gain, group_router, expert_router, w_gate, w_up, w_down, out_gain,
    out, gate_w, up_w, down_w, rows, turned, hidden, held, core_out, core_in, side_out, side_in,
    line_out, up_in, down_in, squares, total,
    load_sem, row_sent, row_got, core_sent, core_got, side_sent, side_got,
    line_sent, up_got, down_got, square_sent, square_got,
):
    tok_dev, width = tokens.shape
    experts = expert_router.shape[0]
    groups = group_router.shape[0]
    sides = 2 if (n // CORES) % 2 == 0 else 1
    plane = sides * CORES
    depth = n // plane
    ntok = n * tok_dev
    block = width // n
    ff = gate_w.shape[1]
    me = lax.axis_index("ep")
    z, y, c = me // plane, (me // CORES) % sides, me % CORES
    side_step, core_step = (1 - 2 * y) * CORES, 1 - 2 * c

    loads = [
        pltpu.make_async_copy(src.at[0], dst, load_sem.at[i])
        for i, (src, dst) in enumerate(((w_gate, gate_w), (w_up, up_w), (w_down, down_w)))
    ]
    for load in loads:
        load.start()

    barrier = pltpu.get_barrier_semaphore()

    def greet(k, carry):
        pl.semaphore_signal(
            barrier, inc=1, device_id={"ep": (me + k) % n}, device_id_type=pl.DeviceIdType.MESH
        )
        return carry

    lax.fori_loop(1, n, greet, 0)

    values = tokens[...].astype(jnp.float32)
    scaled = values * lax.rsqrt(jnp.mean(values * values, axis=1, keepdims=True) + EPSILON)
    normed = (scaled * in_gain[...]).astype(jnp.bfloat16)
    rows[me, :, :width] = normed
    wide = normed.astype(jnp.float32)
    across = (((1,), (1,)), ((), ()))
    group_logit = lax.dot_general(
        group_router[...], wide, across, precision=HIGH, preferred_element_type=jnp.float32
    )
    expert_logit = lax.dot_general(
        expert_router[...], wide, across, precision=HIGH, preferred_element_type=jnp.float32
    )
    group_exp = jnp.exp(group_logit)
    group_prob = group_exp / jnp.sum(group_exp, axis=0, keepdims=True)
    number = lax.broadcasted_iota(jnp.int32, (experts, tok_dev), 0)
    named = number == routes[0:1, :]
    for j in range(1, routes.shape[0]):
        named = named | (number == routes[j : j + 1, :])
    chosen = jnp.where(named, jnp.exp(expert_logit), 0.0)
    weight = chosen / jnp.sum(chosen, axis=0, keepdims=True)
    per_group = experts // groups
    of_group = jnp.zeros_like(weight)
    for g in range(groups):
        inside = (number >= g * per_group) & (number < (g + 1) * per_group)
        of_group = jnp.where(inside, group_prob[g : g + 1, :], of_group)
    weight = weight * of_group
    high = weight.astype(jnp.bfloat16).astype(jnp.float32)
    turned[...] = jnp.zeros_like(turned)
    turned[:experts, :tok_dev] = high
    turned[experts : 2 * experts, :tok_dev] = weight - high
    rows[me, :, width:] = turned[...].T[:tok_dev, :].astype(jnp.bfloat16)

    pl.semaphore_wait(barrier, n - 1)

    def row_copy(slot, way, device):
        return pltpu.make_async_remote_copy(
            src_ref=rows.at[slot], dst_ref=rows.at[slot],
            send_sem=row_sent.at[way, slot], recv_sem=row_got.at[slot],
            device_id={"ep": device}, device_id_type=pl.DeviceIdType.MESH,
        )

    def to_side(slot):
        if sides > 1:
            row_copy(slot, SIDE, me + side_step).start()

    def to_core(slot):
        row_copy(slot, CORE, me + core_step).start()

    def to_up(slot):
        @pl.when(z < depth - 1)
        def _():
            row_copy(slot, UP, me + plane).start()

    def to_down(slot):
        @pl.when(z > 0)
        def _():
            row_copy(slot, DOWN, me - plane).start()

    def got(slot):
        row_copy(slot, CORE, me + core_step).wait_recv()

    to_up(me)
    to_down(me)
    to_side(me)
    to_core(me)

    def from_side(k):
        if sides > 1:
            @pl.when(z - k >= 0)
            def _():
                slot = me - k * plane + side_step
                got(slot)
                to_core(slot)

            if k > 0:
                @pl.when(z + k < depth)
                def _():
                    slot = me + k * plane + side_step
                    got(slot)
                    to_core(slot)

    for k in range(1, depth):
        @pl.when(z - k >= 0)
        def _():
            slot = me - k * plane
            got(slot)
            to_up(slot)
            to_side(slot)
            to_core(slot)

        @pl.when(z + k < depth)
        def _():
            slot = me + k * plane
            got(slot)
            to_down(slot)
            to_side(slot)
            to_core(slot)

        from_side(k - 1)
    from_side(depth - 1)

    def from_core(k, carry):
        got(k * CORES + 1 - c)
        return carry

    lax.fori_loop(0, n // CORES, from_core, 0)

    loads[0].wait()
    loads[1].wait()
    lane = lax.broadcasted_iota(jnp.int32, (ntok, LANES), 1)
    mine = (lane == me) | (lane == experts + me)
    spread = rows[:, :, width:].reshape(ntok, LANES).astype(jnp.float32)
    column = jnp.sum(jnp.where(mine, spread, 0.0), axis=1, keepdims=True)
    tile = min(256, ff)

    def forward(i, carry):
        at = pl.ds(pl.multiple_of(i * tile, tile), tile)
        arrived = rows[:, :, :width].reshape(ntok, width)
        gate = jnp.dot(arrived, gate_w[:, at], preferred_element_type=jnp.float32)
        upward = jnp.dot(arrived, up_w[:, at], preferred_element_type=jnp.float32)
        silu = gate / (1.0 + jnp.exp(-gate))
        hidden[:, at] = (silu * upward * column).astype(jnp.bfloat16)
        return carry

    lax.fori_loop(0, ff // tile, forward, 0)
    loads[2].wait()

    def core_copy(j):
        return pltpu.make_async_remote_copy(
            src_ref=core_out.at[j], dst_ref=core_in.at[j],
            send_sem=core_sent.at[j], recv_sem=core_got.at[j],
            device_id={"ep": me + core_step}, device_id_type=pl.DeviceIdType.MESH,
        )

    def side_copy(j):
        return pltpu.make_async_remote_copy(
            src_ref=side_out.at[j], dst_ref=side_in.at[j],
            send_sem=side_sent.at[j], recv_sem=side_got.at[j],
            device_id={"ep": me + side_step}, device_id_type=pl.DeviceIdType.MESH,
        )

    def up_copy(target):
        return pltpu.make_async_remote_copy(
            src_ref=line_out.at[target], dst_ref=up_in.at[target],
            send_sem=line_sent.at[target], recv_sem=up_got.at[target],
            device_id={"ep": me + plane}, device_id_type=pl.DeviceIdType.MESH,
        )

    def down_copy(target):
        return pltpu.make_async_remote_copy(
            src_ref=line_out.at[target], dst_ref=down_in.at[target],
            send_sem=line_sent.at[target], recv_sem=down_got.at[target],
            device_id={"ep": me - plane}, device_id_type=pl.DeviceIdType.MESH,
        )

    def produce(j):
        span = plane * block
        at = pl.ds(pl.multiple_of(target_of(j, z, depth) * span, span), span)
        answer = jnp.dot(hidden[...], down_w[:, at], preferred_element_type=jnp.float32)
        for s in range(sides):
            first = answer[:, s * CORES * block : (s * CORES + 1) * block]
            second = answer[:, (s * CORES + 1) * block : (s + 1) * CORES * block]
            held[j, s] = jnp.where(c == 0, first, second)
            core_out[j, s] = jnp.where(c == 0, second, first).astype(jnp.bfloat16)
        core_copy(j).start()

    def pair(j):
        core_copy(j).wait_recv()
        held[j, y] = held[j, y] + core_in[j, y].astype(jnp.float32)
        if sides > 1:
            far = held[j, 1 - y] + core_in[j, 1 - y].astype(jnp.float32)
            side_out[j] = far.astype(jnp.bfloat16)
            side_copy(j).start()

    produce(0)

    def produce_pair(j, carry):
        produce(j)
        pair(j - 1)
        return carry

    lax.fori_loop(1, depth, produce_pair, 0)
    pair(depth - 1)

    def plane_sum(j):
        found = held[j, y]
        if sides > 1:
            side_copy(j).wait_recv()
            found = found + side_in[j].astype(jnp.float32)
        return found

    def line(j, carry):
        target = target_of(j, z, depth)
        held[j, y] = plane_sum(j)

        @pl.when(target > z)
        def _():
            @pl.when(z > 0)
            def _():
                up_copy(target).wait_recv()
                held[j, y] = held[j, y] + up_in[target].astype(jnp.float32)

            line_out[target] = held[j, y].astype(jnp.bfloat16)
            up_copy(target).start()

        @pl.when(target < z)
        def _():
            @pl.when(z < depth - 1)
            def _():
                down_copy(target).wait_recv()
                held[j, y] = held[j, y] + down_in[target].astype(jnp.float32)

            line_out[target] = held[j, y].astype(jnp.bfloat16)
            down_copy(target).start()

        return carry

    lax.fori_loop(0, depth - 1, line, 0)
    total[...] = plane_sum(depth - 1)

    @pl.when(z > 0)
    def _():
        up_copy(z).wait_recv()
        total[...] = total[...] + up_in[z].astype(jnp.float32)

    @pl.when(z < depth - 1)
    def _():
        down_copy(z).wait_recv()
        total[...] = total[...] + down_in[z].astype(jnp.float32)

    mixed = total[...]
    summed = lax.dot_general(
        jnp.ones((8, block), jnp.float32), mixed * mixed, across,
        precision=HIGH, preferred_element_type=jnp.float32,
    )
    squares[me] = summed[0:1, :]

    def square_copy(slot, device):
        return pltpu.make_async_remote_copy(
            src_ref=squares.at[slot], dst_ref=squares.at[slot],
            send_sem=square_sent.at[device], recv_sem=square_got.at[slot],
            device_id={"ep": device}, device_id_type=pl.DeviceIdType.MESH,
        )

    def square_start(k, carry):
        square_copy(me, (me + k) % n).start()
        return carry

    lax.fori_loop(1, n, square_start, 0)

    def row_done(k, carry):
        slot = k * plane + y * CORES + c
        row_copy(slot, CORE, me + core_step).wait_send()
        if sides > 1:
            row_copy(slot, SIDE, me + side_step).wait_send()
            row_copy(slot + side_step, CORE, me + core_step).wait_send()

        @pl.when((k <= z) & (z < depth - 1))
        def _():
            row_copy(slot, UP, me + plane).wait_send()

        @pl.when((k >= z) & (z > 0))
        def _():
            row_copy(slot, DOWN, me - plane).wait_send()

        core_copy(k).wait_send()
        if sides > 1:
            side_copy(k).wait_send()

        @pl.when(k > z)
        def _():
            up_copy(k).wait_send()

        @pl.when(k < z)
        def _():
            down_copy(k).wait_send()

        return carry

    lax.fori_loop(0, depth, row_done, 0)

    def square_wait(k, carry):
        square_copy((me + k) % n, (me + k) % n).wait_recv()
        return carry

    lax.fori_loop(1, n, square_wait, 0)
    power = jnp.sum(squares[...], axis=0)
    tall = jnp.broadcast_to(power, (LANES, ntok)).T[:, :block]
    scale = lax.rsqrt(tall / width + EPSILON)
    out[...] = (total[...] * scale * out_gain[...]).astype(jnp.bfloat16)

    def square_done(k, carry):
        square_copy(me, (me + k) % n).wait_send()
        return carry

    lax.fori_loop(1, n, square_done, 0)


def per_device(
    n, tokens, routes, in_gain, group_router, expert_router, w_gate, w_up, w_down, out_gain
):
    tok_dev, width = tokens.shape
    ff = w_gate.shape[2]
    ntok, block = n * tok_dev, width // n
    sides = 2 if (n // CORES) % 2 == 0 else 1
    depth = n // (sides * CORES)
    bf16, f32 = jnp.bfloat16, jnp.float32
    dma = pltpu.SemaphoreType.DMA
    vmem = pl.BlockSpec(memory_space=pltpu.VMEM)
    hbm = pl.BlockSpec(memory_space=pl.ANY)
    return pl.pallas_call(
        functools.partial(kernel, n),
        out_shape=jax.ShapeDtypeStruct((ntok, block), bf16),
        in_specs=[vmem] * 5 + [hbm] * 3 + [vmem],
        out_specs=vmem,
        scratch_shapes=[
            pltpu.VMEM((width, ff), bf16),
            pltpu.VMEM((width, ff), bf16),
            pltpu.VMEM((ff, width), bf16),
            pltpu.VMEM((n, tok_dev, width + LANES), bf16),
            pltpu.VMEM((LANES, LANES), f32),
            pltpu.VMEM((ntok, ff), bf16),
            pltpu.VMEM((depth, sides, ntok, block), f32),
            pltpu.VMEM((depth, sides, ntok, block), bf16),
            pltpu.VMEM((depth, sides, ntok, block), bf16),
            pltpu.VMEM((depth, ntok, block), bf16),
            pltpu.VMEM((depth, ntok, block), bf16),
            pltpu.VMEM((depth, ntok, block), bf16),
            pltpu.VMEM((depth, ntok, block), bf16),
            pltpu.VMEM((depth, ntok, block), bf16),
            pltpu.VMEM((n, 1, ntok), f32),
            pltpu.VMEM((ntok, block), f32),
            dma((3,)),
            dma((4, n)),
            dma((n,)),
            dma((depth,)),
            dma((depth,)),
            dma((depth,)),
            dma((depth,)),
            dma((depth,)),
            dma((depth,)),
            dma((depth,)),
            dma((n,)),
            dma((n,)),
        ],
        compiler_params=pltpu.CompilerParams(
            collective_id=0, has_side_effects=True, vmem_limit_bytes=60 * 1024 * 1024
        ),
    )(
        tokens, routes.T, in_gain.reshape(1, width), group_router.T, expert_router.T,
        w_gate, w_up, w_down, out_gain.reshape(1, block),
    )


def solution(mesh):
    in_specs = (
        P(("grp", "ep"), None),
        P(("grp", "ep"), None),
        P(),
        P(),
        P(),
        P("ep", None, None),
        P("ep", None, None),
        P("ep", None, None),
        P("ep"),
    )
    return jax.shard_map(
        functools.partial(per_device, mesh.shape["ep"]),
        mesh=mesh, in_specs=in_specs, out_specs=P("grp", "ep"), check_vma=False,
    )
```

time: 95.7 us -> 56.5 us (0.59)
  Pallas kernels: 0 us -> 54.8 us
  blocking collectives: 48.6 us -> 0 us
  waiting for transfers between devices: 18.6 us -> 0 us
  local copies, waits for them, and re-layouts: 11.5 us -> 1.57 us
  matrix products: 5.99 us -> 0 us
  other arithmetic: 5.19 us -> 0 us
  starting transfers between devices: 5.15 us -> 0 us
    pallas_call x0 -> x1, Pallas kernels: none -> 54.8 us  [per_device(): pl.pallas_call(functools.partial(kernel, n), out_shape=jax.ShapeDtypeStru...]
    all_to_all x2 -> x0, blocking collectives: 48.6 us -> none  [the longest x1 32 us: per_device(): lax.all_to_all(outgoing, 'ep', split_axis=0, concat_axis=0, tiled=True)]
    all_to_all x1 -> x0, waiting for transfers between devices: 18.6 us -> none  [per_device(): lax.all_to_all(answer, 'ep', split_axis=0, concat_axis=0, tiled=True)]
    gather x12 -> x0, local copies, waits for them, and re-layouts: 6.68 us -> none  [the longest x5 1.88 us: gate_values(): jnp.take_along_axis(group_prob, routes // per_group, axis=1) * expert_prob]
    dot_general x4 -> x0, matrix products: 5.99 us -> none  [the longest x1 4.01 us: expert_rows(): jnp.dot(hidden, w_down[0], preferred_element_type=jnp.float32)]
    all_to_all x1 -> x0, starting transfers between devices: 5.15 us -> none  [per_device(): lax.all_to_all(answer, 'ep', split_axis=0, concat_axis=0, tiled=True)]
    reduce_sum x5 -> x0, other arithmetic: 2.1 us -> none  [the longest x1 1.04 us: normalize(): jnp.mean(values * values, axis=1, keepdims=True) + EPSILON]
    scatter x2 -> x0, local copies, waits for them, and re-layouts: 1.99 us -> none  [the longest x1 1.01 us: per_device(): jnp.zeros((experts * capacity,), jnp.bool_).at[slot_index].set(True)]
  transfers between devices with their start and end apart: 1 -> 0, of which waited for: 1 -> 0; matrix products, arithmetic and copies ran while one was open for 4% -> 0% of each run, Pallas kernels for 0% -> 0%
where the time goes in v1:
time: 56.5 us; the launch traced here: 56.4 us
  Pallas kernels  54.8 us (97%)
  local copies, waits for them, and re-layouts  1.57 us (3%)
    pallas_call x1, Pallas kernels, per_device(): pl.pallas_call(functools.partial(kernel, n), out_shape=jax.ShapeDtypeStru...  54.8 us
    unnamed x1, local copies, waits for them, and re-layouts  1.57 us

profile of v1, /device:TPU:0, one launch (start us, length us, event | category | flops | bytes accessed | tf_op | source)
XLA Modules:
  0.0 56.4 jit_solution(553093272628702028)
XLA Ops:
  0.0 54.8 %shard_map.91 = bf16[512,128]{1,0:T(8,128)(2,1)} custom-call(bf16[32,2048]{1,0:T(8,128)(2,1)} %tokens.1, s32[4,32]{1,0:T(4,128)} %bitcast.8, f32[1,2048]{1,0:T(1,128)} %bitcast.7, f32[4,2048]{1,0:T(4,128)} %bitcast.6, f32[16,2048]{1,0:T(8,128)} %bitcast.5, bf16[1,2048,512]{2,1,0:T(8,128)(2,1)} %w_gate.1, bf16[1,2048,512]{2,1,0:T(8,128)(2,1)} %w_up.1, ...), custom_call_target="tpu_custom_call" | custom-call | tf_op jit(solution)/shard_map/pallas_call | solution.py:375
  54.8 1.6 %copy.11 = bf16[512,128]{1,0:T(8,128)(2,1)} copy(bf16[512,128]{1,0:T(8,128)(2,1)} %shard_map.91) | data formatting | bytes 262144

commit v2 on v1

--- a/solution.py
+++ b/solution.py
@@ -12,6 +12,8 @@
 CORES = 2
 HIGH = lax.Precision.HIGHEST
 UP, DOWN, SIDE, CORE = 0, 1, 2, 3
+ROW_PIECES = 2
+SUM_PIECES = 2
 
 
 def target_of(step, z, depth):
@@ -41,6 +43,8 @@
     ntok = n * tok_dev
     block = width // n
     ff = gate_w.shape[1]
+    piece = tok_dev // ROW_PIECES
+    part = ntok // SUM_PIECES
     me = lax.axis_index("ep")
     z, y, c = me // plane, (me // CORES) % sides, me % CORES
     side_step, core_step = (1 - 2 * y) * CORES, 1 - 2 * c
@@ -96,75 +100,83 @@
 
     pl.semaphore_wait(barrier, n - 1)
 
-    def row_copy(slot, way, device):
-        return pltpu.make_async_remote_copy(
-            src_ref=rows.at[slot], dst_ref=rows.at[slot],
-            send_sem=row_sent.at[way, slot], recv_sem=row_got.at[slot],
+    def row_copy(slot, p, way, device):
+        at = rows.at[slot, pl.ds(p * piece, piece)]
+        return pltpu.make_async_remote_copy(
+            src_ref=at, dst_ref=at,
+            send_sem=row_sent.at[way, slot, p], recv_sem=row_got.at[slot, p],
             device_id={"ep": device}, device_id_type=pl.DeviceIdType.MESH,
         )
 
-    def to_side(slot):
+    def to_side(slot, p):
         if sides > 1:
-            row_copy(slot, SIDE, me + side_step).start()
-
-    def to_core(slot):
-        row_copy(slot, CORE, me + core_step).start()
-
-    def to_up(slot):
+            row_copy(slot, p, SIDE, me + side_step).start()
+
+    def to_core(slot, p):
+        row_copy(slot, p, CORE, me + core_step).start()
+
+    def to_up(slot, p):
         @pl.when(z < depth - 1)
         def _():
-            row_copy(slot, UP, me + plane).start()
-
-    def to_down(slot):
+            row_copy(slot, p, UP, me + plane).start()
+
+    def to_down(slot, p):
         @pl.when(z > 0)
         def _():
-            row_copy(slot, DOWN, me - plane).start()
-
-    def got(slot):
-        row_copy(slot, CORE, me + core_step).wait_recv()
-
-    to_up(me)
-    to_down(me)
-    to_side(me)
-    to_core(me)
-
-    def from_side(k):
+            row_copy(slot, p, DOWN, me - plane).start()
+
+    def got(slot, p):
+        row_copy(slot, p, CORE, me + core_step).wait_recv()
+
+    for p in range(ROW_PIECES):
+        to_up(me, p)
+        to_down(me, p)
+        to_side(me, p)
+    for p in range(ROW_PIECES):
+        to_core(me, p)
+
+    def from_side(k, p):
         if sides > 1:
             @pl.when(z - k >= 0)
             def _():
                 slot = me - k * plane + side_step
-                got(slot)
-                to_core(slot)
+                got(slot, p)
+                to_core(slot, p)
 
             if k > 0:
                 @pl.when(z + k < depth)
                 def _():
                     slot = me + k * plane + side_step
-                    got(slot)
-                    to_core(slot)
+                    got(slot, p)
+                    to_core(slot, p)
 
     for k in range(1, depth):
-        @pl.when(z - k >= 0)
-        def _():
-            slot = me - k * plane
-            got(slot)
-            to_up(slot)
-            to_side(slot)
-            to_core(slot)
-
-        @pl.when(z + k < depth)
-        def _():
-            slot = me + k * plane
-            got(slot)
-            to_down(slot)
-            to_side(slot)
-            to_core(slot)
-
-        from_side(k - 1)
-    from_side(depth - 1)
+        for p in range(ROW_PIECES):
+            @pl.when(z - k >= 0)
+            def _():
+                slot = me - k * plane
+                got(slot, p)
+                to_up(slot, p)
+                to_side(slot, p)
+                to_core(slot, p)
+
+            @pl.when(z + k < depth)
+            def _():
+                slot = me + k * plane
+                got(slot, p)
+                to_down(slot, p)
+                to_side(slot, p)
+                to_core(slot, p)
+
+            if k > 1:
+                from_side(k - 2, p)
+    for k in range(max(depth - 2, 0), depth):
+        for p in range(ROW_PIECES):
+            from_side(k, p)
 
     def from_core(k, carry):
-        got(k * CORES + 1 - c)
+        for p in range(ROW_PIECES):
+            got(k * CORES + 1 - c, p)
         return carry
 
     lax.fori_loop(0, n // CORES, from_core, 0)
@@ -217,80 +229,88 @@
             device_id={"ep": me - plane}, device_id_type=pl.DeviceIdType.MESH,
         )
 
-    def produce(j):
+    units = depth * SUM_PIECES
+
+    def produce(u):
         span = plane * block
-        at = pl.ds(pl.multiple_of(target_of(j, z, depth) * span, span), span)
-        answer = jnp.dot(hidden[...], down_w[:, at], preferred_element_type=jnp.float32)
+        target = target_of(u // SUM_PIECES, z, depth)
+        at = pl.ds(pl.multiple_of(target * span, span), span)
+        some = pl.ds(pl.multiple_of(u % SUM_PIECES * part, part), part)
+        answer = jnp.dot(hidden[some, :], down_w[:, at], preferred_element_type=jnp.float32)
         for s in range(sides):
             first = answer[:, s * CORES * block : (s * CORES + 1) * block]
             second = answer[:, (s * CORES + 1) * block : (s + 1) * CORES * block]
-            held[j, s] = jnp.where(c == 0, first, second)
-            core_out[j, s] = jnp.where(c == 0, second, first).astype(jnp.bfloat16)
-        core_copy(j).start()
-
-    def pair(j):
-        core_copy(j).wait_recv()
-        held[j, y] = held[j, y] + core_in[j, y].astype(jnp.float32)
+            held[u, s] = jnp.where(c == 0, first, second)
+            core_out[u, s] = jnp.where(c == 0, second, first).astype(jnp.bfloat16)
+        core_copy(u).start()
+
+    def pair(u):
+        core_copy(u).wait_recv()
+        held[u, y] = held[u, y] + core_in[u, y].astype(jnp.float32)
         if sides > 1:
-            far = held[j, 1 - y] + core_in[j, 1 - y].astype(jnp.float32)
-            side_out[j] = far.astype(jnp.bfloat16)
-            side_copy(j).start()
+            far = held[u, 1 - y] + core_in[u, 1 - y].astype(jnp.float32)
+            side_out[u] = far.astype(jnp.bfloat16)
+            side_copy(u).start()
 
     produce(0)
 
-    def produce_pair(j, carry):
-        produce(j)
-        pair(j - 1)
-        return carry
-
-    lax.fori_loop(1, depth, produce_pair, 0)
-    pair(depth - 1)
-
-    def plane_sum(j):
-        found = held[j, y]
+    def produce_pair(u, carry):
+        produce(u)
+        pair(u - 1)
+        return carry
+
+    lax.fori_loop(1, units, produce_pair, 0)
+    pair(units - 1)
+
+    def plane_sum(u):
+        found = held[u, y]
         if sides > 1:
-            side_copy(j).wait_recv()
-            found = found + side_in[j].astype(jnp.float32)
+            side_copy(u).wait_recv()
+            found = found + side_in[u].astype(jnp.float32)
         return found
 
-    def line(j, carry):
-        target = target_of(j, z, depth)
-        held[j, y] = plane_sum(j)
+    def line(u, carry):
+        target = target_of(u // SUM_PIECES, z, depth)
+        spot = target * SUM_PIECES + u % SUM_PIECES
+        held[u, y] = plane_sum(u)
 
         @pl.when(target > z)
         def _():
             @pl.when(z > 0)
             def _():
-                up_copy(target).wait_recv()
-                held[j, y] = held[j, y] + up_in[target].astype(jnp.float32)
-
-            line_out[target] = held[j, y].astype(jnp.bfloat16)
-            up_copy(target).start()
+                up_copy(spot).wait_recv()
+                held[u, y] = held[u, y] + up_in[spot].astype(jnp.float32)
+
+            line_out[spot] = held[u, y].astype(jnp.bfloat16)
+            up_copy(spot).start()
 
         @pl.when(target < z)
         def _():
             @pl.when(z < depth - 1)
             def _():
-                down_copy(target).wait_recv()
-                held[j, y] = held[j, y] + down_in[target].astype(jnp.float32)
-
-            line_out[target] = held[j, y].astype(jnp.bfloat16)
-            down_copy(target).start()
-
-        return carry
-
-    lax.fori_loop(0, depth - 1, line, 0)
-    total[...] = plane_sum(depth - 1)
-
-    @pl.when(z > 0)
-    def _():
-        up_copy(z).wait_recv()
-        total[...] = total[...] + up_in[z].astype(jnp.float32)
-
-    @pl.when(z < depth - 1)
-    def _():
-        down_copy(z).wait_recv()
-        total[...] = total[...] + down_in[z].astype(jnp.float32)
+                down_copy(spot).wait_recv()
+                held[u, y] = held[u, y] + down_in[spot].astype(jnp.float32)
+
+            line_out[spot] = held[u, y].astype(jnp.bfloat16)
+            down_copy(spot).start()
+
+        return carry
+
+    lax.fori_loop(0, units - SUM_PIECES, line, 0)
+    for p in range(SUM_PIECES):
+        spot = z * SUM_PIECES + p
+        some = pl.ds(p * part, part)
+        total[some, :] = plane_sum(units - SUM_PIECES + p)
+
+        @pl.when(z > 0)
+        def _():
+            up_copy(spot).wait_recv()
+            total[some, :] = total[some, :] + up_in[spot].astype(jnp.float32)
+
+        @pl.when(z < depth - 1)
+        def _():
+            down_copy(spot).wait_recv()
+            total[some, :] = total[some, :] + down_in[spot].astype(jnp.float32)
 
     mixed = total[...]
     summed = lax.dot_general(
@@ -314,34 +334,41 @@
 
     def row_done(k, carry):
         slot = k * plane + y * CORES + c
-        row_copy(slot, CORE, me + core_step).wait_send()
+        for p in range(ROW_PIECES):
+            row_copy(slot, p, CORE, me + core_step).wait_send()
+            if sides > 1:
+                row_copy(slot, p, SIDE, me + side_step).wait_send()
+                row_copy(slot + side_step, p, CORE, me + core_step).wait_send()
+
+            @pl.when((k <= z) & (z < depth - 1))
+            def _():
+                row_copy(slot, p, UP, me + plane).wait_send()
+
+            @pl.when((k >= z) & (z > 0))
+            def _():
+                row_copy(slot, p, DOWN, me - plane).wait_send()
+
+        return carry
+
+    lax.fori_loop(0, depth, row_done, 0)
+
+    def sum_done(u, carry):
+        k = u // SUM_PIECES
+        core_copy(u).wait_send()
         if sides > 1:
-            row_copy(slot, SIDE, me + side_step).wait_send()
-            row_copy(slot + side_step, CORE, me + core_step).wait_send()
-
-        @pl.when((k <= z) & (z < depth - 1))
-        def _():
-            row_copy(slot, UP, me + plane).wait_send()
-
-        @pl.when((k >= z) & (z > 0))
-        def _():
-            row_copy(slot, DOWN, me - plane).wait_send()
-
-        core_copy(k).wait_send()
-        if sides > 1:
-            side_copy(k).wait_send()
+            side_copy(u).wait_send()
 
         @pl.when(k > z)
         def _():
-            up_copy(k).wait_send()
+            up_copy(u).wait_send()
 
         @pl.when(k < z)
         def _():
-            down_copy(k).wait_send()
-
-        return carry
-
-    lax.fori_loop(0, depth, row_done, 0)
+            down_copy(u).wait_send()
+
+        return carry
+
+    lax.fori_loop(0, depth * SUM_PIECES, sum_done, 0)
 
     def square_wait(k, carry):
         square_copy((me + k) % n, (me + k) % n).wait_recv()
@@ -367,7 +394,8 @@
     ff = w_gate.shape[2]
     ntok, block = n * tok_dev, width // n
     sides = 2 if (n // CORES) % 2 == 0 else 1
-    depth = n // (sides * CORES)
+    units = n // (sides * CORES) * SUM_PIECES
+    part = ntok // SUM_PIECES
     bf16, f32 = jnp.bfloat16, jnp.float32
     dma = pltpu.SemaphoreType.DMA
     vmem = pl.BlockSpec(memory_space=pltpu.VMEM)
@@ -384,26 +412,26 @@
             pltpu.VMEM((n, tok_dev, width + LANES), bf16),
             pltpu.VMEM((LANES, LANES), f32),
             pltpu.VMEM((ntok, ff), bf16),
-            pltpu.VMEM((depth, sides, ntok, block), f32),
-            pltpu.VMEM((depth, sides, ntok, block), bf16),
-            pltpu.VMEM((depth, sides, ntok, block), bf16),
-            pltpu.VMEM((depth, ntok, block), bf16),
-            pltpu.VMEM((depth, ntok, block), bf16),
-            pltpu.VMEM((depth, ntok, block), bf16),
-            pltpu.VMEM((depth, ntok, block), bf16),
-            pltpu.VMEM((depth, ntok, block), bf16),
+            pltpu.VMEM((units, sides, part, block), f32),
+            pltpu.VMEM((units, sides, part, block), bf16),
+            pltpu.VMEM((units, sides, part, block), bf16),
+            pltpu.VMEM((units, part, block), bf16),
+            pltpu.VMEM((units, part, block), bf16),
+            pltpu.VMEM((units, part, block), bf16),
+            pltpu.VMEM((units, part, block), bf16),
+            pltpu.VMEM((units, part, block), bf16),
             pltpu.VMEM((n, 1, ntok), f32),
             pltpu.VMEM((ntok, block), f32),
             dma((3,)),
-            dma((4, n)),
-            dma((n,)),
-            dma((depth,)),
-            dma((depth,)),
-            dma((depth,)),
-            dma((depth,)),
-            dma((depth,)),
-            dma((depth,)),
-            dma((depth,)),
+            dma((4, n, ROW_PIECES)),
+            dma((n, ROW_PIECES)),
+            dma((units,)),
+            dma((units,)),
+            dma((units,)),
+            dma((units,)),
+            dma((units,)),
+            dma((units,)),
+            dma((units,)),
             dma((n,)),
             dma((n,)),
         ],

time: 56.5 us -> 53.9 us (0.954)
  Pallas kernels: 54.8 us -> 52.2 us
    pallas_call x1, Pallas kernels: 54.8 us -> 52.2 us  [per_device(): pl.pallas_call(functools.partial(kernel, n), out_shape=jax.ShapeDtypeStru...]
where the time goes in v2:
time: 53.9 us; the launch traced here: 53.7 us
  Pallas kernels  52.2 us (97%)
  local copies, waits for them, and re-layouts  1.57 us (3%)
    pallas_call x1, Pallas kernels, per_device(): pl.pallas_call(functools.partial(kernel, n), out_shape=jax.ShapeDtypeStru...  52.2 us
    unnamed x1, local copies, waits for them, and re-layouts  1.57 us

profile of v2, /device:TPU:0, one launch (start us, length us, event | category | flops | bytes accessed | tf_op | source)
XLA Modules:
  0.0 53.7 jit_solution(13150571320907553089)
XLA Ops:
  0.0 52.2 %shard_map.91 = bf16[512,128]{1,0:T(8,128)(2,1)} custom-call(bf16[32,2048]{1,0:T(8,128)(2,1)} %tokens.1, s32[4,32]{1,0:T(4,128)} %bitcast.8, f32[1,2048]{1,0:T(1,128)} %bitcast.7, f32[4,2048]{1,0:T(4,128)} %bitcast.6, f32[16,2048]{1,0:T(8,128)} %bitcast.5, bf16[1,2048,512]{2,1,0:T(8,128)(2,1)} %w_gate.1, bf16[1,2048,512]{2,1,0:T(8,128)(2,1)} %w_up.1, ...), custom_call_target="tpu_custom_call" | custom-call | tf_op jit(solution)/shard_map/pallas_call | solution.py:403
  52.2 1.6 %copy.11 = bf16[512,128]{1,0:T(8,128)(2,1)} copy(bf16[512,128]{1,0:T(8,128)(2,1)} %shard_map.91) | data formatting | bytes 262144

commit v3 on v2

--- a/solution.py
+++ b/solution.py
@@ -14,6 +14,7 @@
 UP, DOWN, SIDE, CORE = 0, 1, 2, 3
 ROW_PIECES = 2
 SUM_PIECES = 2
+AHEAD = 3
 
 
 def target_of(step, z, depth):
@@ -58,13 +59,22 @@
 
     barrier = pltpu.get_barrier_semaphore()
 
-    def greet(k, carry):
+    def greet(device):
         pl.semaphore_signal(
-            barrier, inc=1, device_id={"ep": (me + k) % n}, device_id_type=pl.DeviceIdType.MESH
-        )
-        return carry
-
-    lax.fori_loop(1, n, greet, 0)
+            barrier, inc=1, device_id={"ep": device}, device_id_type=pl.DeviceIdType.MESH
+        )
+
+    greet(me + core_step)
+    if sides > 1:
+        greet(me + side_step)
+
+    @pl.when(z < depth - 1)
+    def _():
+        greet(me + plane)
+
+    @pl.when(z > 0)
+    def _():
+        greet(me - plane)
 
     values = tokens[...].astype(jnp.float32)
     scaled = values * lax.rsqrt(jnp.mean(values * values, axis=1, keepdims=True) + EPSILON)
@@ -98,7 +108,7 @@
     turned[experts : 2 * experts, :tok_dev] = weight - high
     rows[me, :, width:] = turned[...].T[:tok_dev, :].astype(jnp.bfloat16)
 
-    pl.semaphore_wait(barrier, n - 1)
+    pl.semaphore_wait(barrier, sides + jnp.where(z > 0, 1, 0) + jnp.where(z < depth - 1, 1, 0))
 
     def row_copy(slot, p, way, device):
         at = rows.at[slot, pl.ds(p * piece, piece)]
@@ -252,15 +262,24 @@
             side_out[u] = far.astype(jnp.bfloat16)
             side_copy(u).start()
 
-    produce(0)
+    ahead = min(AHEAD, units)
+
+    def produce_only(u, carry):
+        produce(u)
+        return carry
 
     def produce_pair(u, carry):
         produce(u)
-        pair(u - 1)
-        return carry
-
-    lax.fori_loop(1, units, produce_pair, 0)
-    pair(units - 1)
+        pair(u - ahead)
+        return carry
+
+    def pair_only(u, carry):
+        pair(u)
+        return carry
+
+    lax.fori_loop(0, ahead, produce_only, 0)
+    lax.fori_loop(ahead, units, produce_pair, 0)
+    lax.fori_loop(units - ahead, units, pair_only, 0)
 
     def plane_sum(u):
         found = held[u, y]

time: 53.9 us -> 50.8 us (0.942)
  Pallas kernels: 52.2 us -> 49.1 us
    pallas_call x1, Pallas kernels: 52.2 us -> 49.1 us  [per_device(): pl.pallas_call(functools.partial(kernel, n), out_shape=jax.ShapeDtypeStru...]
where the time goes in v3:
time: 50.8 us; the launch traced here: 50.6 us
  Pallas kernels  49.1 us (97%)
  local copies, waits for them, and re-layouts  1.57 us (3%)
    pallas_call x1, Pallas kernels, per_device(): pl.pallas_call(functools.partial(kernel, n), out_shape=jax.ShapeDtypeStru...  49.1 us
    unnamed x1, local copies, waits for them, and re-layouts  1.57 us

profile of v3, /device:TPU:0, one launch (start us, length us, event | category | flops | bytes accessed | tf_op | source)
XLA Modules:
  0.0 50.6 jit_solution(2015677869470812003)
XLA Ops:
  0.0 49.1 %shard_map.91 = bf16[512,128]{1,0:T(8,128)(2,1)} custom-call(bf16[32,2048]{1,0:T(8,128)(2,1)} %tokens.1, s32[4,32]{1,0:T(4,128)} %bitcast.8, f32[1,2048]{1,0:T(1,128)} %bitcast.7, f32[4,2048]{1,0:T(4,128)} %bitcast.6, f32[16,2048]{1,0:T(8,128)} %bitcast.5, bf16[1,2048,512]{2,1,0:T(8,128)(2,1)} %w_gate.1, bf16[1,2048,512]{2,1,0:T(8,128)(2,1)} %w_up.1, ...), custom_call_target="tpu_custom_call" | custom-call | tf_op jit(solution)/shard_map/pallas_call | solution.py:422
  49.1 1.6 %copy.11 = bf16[512,128]{1,0:T(8,128)(2,1)} copy(bf16[512,128]{1,0:T(8,128)(2,1)} %shard_map.91) | data formatting | bytes 262144

commit v4 on v3

--- a/solution.py
+++ b/solution.py
@@ -15,6 +15,7 @@
 ROW_PIECES = 2
 SUM_PIECES = 2
 AHEAD = 3
+EARLY = 2
 
 
 def target_of(step, z, depth):
@@ -180,35 +181,39 @@
 
             if k > 1:
                 from_side(k - 2, p)
-    for k in range(max(depth - 2, 0), depth):
-        for p in range(ROW_PIECES):
-            from_side(k, p)
-
-    def from_core(k, carry):
-        for p in range(ROW_PIECES):
-            got(k * CORES + 1 - c, p)
-        return carry
-
-    lax.fori_loop(0, n // CORES, from_core, 0)
+    tile = min(256, ff)
+    chunk = plane * tok_dev
+    lane = lax.broadcasted_iota(jnp.int32, (chunk, LANES), 1)
+    mine = (lane == me) | (lane == experts + me)
+
+    def forward(i, carry):
+        source = target_of(depth - 1 - i, z, depth)
+        for s in range(sides):
+            for p in range(ROW_PIECES):
+                got(source * plane + s * CORES + 1 - c, p)
+        members = pl.ds(source * plane, plane)
+        some = pl.ds(pl.multiple_of(source * chunk, chunk), chunk)
+        spread = rows[members, :, width:].reshape(chunk, LANES).astype(jnp.float32)
+        column = jnp.sum(jnp.where(mine, spread, 0.0), axis=1, keepdims=True)
+        arrived = rows[members, :, :width].reshape(chunk, width)
+        for t in range(ff // tile):
+            at = pl.ds(t * tile, tile)
+            gate = jnp.dot(arrived, gate_w[:, at], preferred_element_type=jnp.float32)
+            upward = jnp.dot(arrived, up_w[:, at], preferred_element_type=jnp.float32)
+            silu = gate / (1.0 + jnp.exp(-gate))
+            hidden[some, at] = (silu * upward * column).astype(jnp.bfloat16)
+        return carry
 
     loads[0].wait()
     loads[1].wait()
-    lane = lax.broadcasted_iota(jnp.int32, (ntok, LANES), 1)
-    mine = (lane == me) | (lane == experts + me)
-    spread = rows[:, :, width:].reshape(ntok, LANES).astype(jnp.float32)
-    column = jnp.sum(jnp.where(mine, spread, 0.0), axis=1, keepdims=True)
-    tile = min(256, ff)
-
-    def forward(i, carry):
-        at = pl.ds(pl.multiple_of(i * tile, tile), tile)
-        arrived = rows[:, :, :width].reshape(ntok, width)
-        gate = jnp.dot(arrived, gate_w[:, at], preferred_element_type=jnp.float32)
-        upward = jnp.dot(arrived, up_w[:, at], preferred_element_type=jnp.float32)
-        silu = gate / (1.0 + jnp.exp(-gate))
-        hidden[:, at] = (silu * upward * column).astype(jnp.bfloat16)
-        return carry
-
-    lax.fori_loop(0, ff // tile, forward, 0)
+    if depth > 1:
+        for p in range(ROW_PIECES):
+            from_side(depth - 2, p)
+    early = min(EARLY, depth - 1)
+    lax.fori_loop(0, early, forward, 0)
+    for p in range(ROW_PIECES):
+        from_side(depth - 1, p)
+    lax.fori_loop(early, depth, forward, 0)
     loads[2].wait()
 
     def core_copy(j):

time: 50.8 us -> 48.8 us (0.961)
  Pallas kernels: 49.1 us -> 47.1 us
    pallas_call x1, Pallas kernels: 49.1 us -> 47.1 us  [per_device(): pl.pallas_call(functools.partial(kernel, n), out_shape=jax.ShapeDtypeStru...]
where the time goes in v4:
time: 48.8 us; the launch traced here: 48.7 us
  Pallas kernels  47.1 us (97%)
  local copies, waits for them, and re-layouts  1.57 us (3%)
    pallas_call x1, Pallas kernels, per_device(): pl.pallas_call(functools.partial(kernel, n), out_shape=jax.ShapeDtypeStru...  47.1 us
    unnamed x1, local copies, waits for them, and re-layouts  1.57 us

profile of v4, /device:TPU:0, one launch (start us, length us, event | category | flops | bytes accessed | tf_op | source)
XLA Modules:
  0.0 48.7 jit_solution(15047435300945249105)
XLA Ops:
  0.0 47.1 %shard_map.91 = bf16[512,128]{1,0:T(8,128)(2,1)} custom-call(bf16[32,2048]{1,0:T(8,128)(2,1)} %tokens.1, s32[4,32]{1,0:T(4,128)} %bitcast.8, f32[1,2048]{1,0:T(1,128)} %bitcast.7, f32[4,2048]{1,0:T(4,128)} %bitcast.6, f32[16,2048]{1,0:T(8,128)} %bitcast.5, bf16[1,2048,512]{2,1,0:T(8,128)(2,1)} %w_gate.1, bf16[1,2048,512]{2,1,0:T(8,128)(2,1)} %w_up.1, ...), custom_call_target="tpu_custom_call" | custom-call | tf_op jit(solution)/shard_map/pallas_call | solution.py:427
  47.1 1.6 %copy.11 = bf16[512,128]{1,0:T(8,128)(2,1)} copy(bf16[512,128]{1,0:T(8,128)(2,1)} %shard_map.91) | data formatting | bytes 262144

commit v5 on v4

--- a/solution.py
+++ b/solution.py
@@ -13,8 +13,8 @@
 HIGH = lax.Precision.HIGHEST
 UP, DOWN, SIDE, CORE = 0, 1, 2, 3
 ROW_PIECES = 2
-SUM_PIECES = 2
-AHEAD = 3
+SUM_PIECES = 4
+AHEAD = 6
 EARLY = 2
 
 

time: 48.8 us -> 48.3 us (0.990)
  Pallas kernels: 47.1 us -> 46.6 us
    pallas_call x1, Pallas kernels: 47.1 us -> 46.6 us  [per_device(): pl.pallas_call(functools.partial(kernel, n), out_shape=jax.ShapeDtypeStru...]
where the time goes in v5:
time: 48.3 us; the launch traced here: 48.2 us
  Pallas kernels  46.6 us (96%)
  local copies, waits for them, and re-layouts  1.57 us (3%)
    pallas_call x1, Pallas kernels, per_device(): pl.pallas_call(functools.partial(kernel, n), out_shape=jax.ShapeDtypeStru...  46.6 us
    unnamed x1, local copies, waits for them, and re-layouts  1.57 us

profile of v5, /device:TPU:0, one launch (start us, length us, event | category | flops | bytes accessed | tf_op | source)
XLA Modules:
  0.0 48.2 jit_solution(1350259169552181243)
XLA Ops:
  0.0 46.6 %shard_map.91 = bf16[512,128]{1,0:T(8,128)(2,1)} custom-call(bf16[32,2048]{1,0:T(8,128)(2,1)} %tokens.1, s32[4,32]{1,0:T(4,128)} %bitcast.8, f32[1,2048]{1,0:T(1,128)} %bitcast.7, f32[4,2048]{1,0:T(4,128)} %bitcast.6, f32[16,2048]{1,0:T(8,128)} %bitcast.5, bf16[1,2048,512]{2,1,0:T(8,128)(2,1)} %w_gate.1, bf16[1,2048,512]{2,1,0:T(8,128)(2,1)} %w_up.1, ...), custom_call_target="tpu_custom_call" | custom-call | tf_op jit(solution)/shard_map/pallas_call | solution.py:427
  46.6 1.6 %copy.11 = bf16[512,128]{1,0:T(8,128)(2,1)} copy(bf16[512,128]{1,0:T(8,128)(2,1)} %shard_map.91) | data formatting | bytes 262144
